TPU v7x, 32 devices: a whole 2x2x4 slice. The times are simulated.
32 devices in a mesh: sp: 8 (over z, x), tp: 4 (over y, core).
Axes of the slice: x: 2, y: 2, z: 4, core: 2. Of those that a mesh axis runs over, the one named last changes fastest.
Arguments:
- queries: bfloat16 [1024, 1024], P('sp', 'tp'), may hold values from -12 to 12
- keys: bfloat16 [1024, 256], P('sp', 'tp'), may hold values from -12 to 12
- values: bfloat16 [1024, 256], P('sp', 'tp'), may hold values from -6 to 6
- log_gate: float32 [16, 1024], P('tp', 'sp'), may hold values from -0.2 to 0, as said below
- log_sum: float32 [16, 1024], P('tp', 'sp'), may hold values from -100 to 100, as said below
- output: bfloat16 [1024, 1024], P('sp', 'tp'), may hold values from -6 to 6
- cotangent: bfloat16 [1024, 1024], P('sp', 'tp'), may hold values from -12 to 12
- normed: bfloat16 [1024, 2048], P('sp', 'tp'), may hold values from -8 to 8
Outputs:
- query_grad: bfloat16 [1024, 1024], P('sp', 'tp')
- key_grad: bfloat16 [1024, 256], P('sp', 'tp')
- value_grad: bfloat16 [1024, 256], P('sp', 'tp')
- weight_grad: float32 [2048, 256], P('sp', 'tp')
Inputs may be any that keep to these rules, and one draw needn't show every extreme that they name: `log_gate`: every entry is negative. log_sum[h, t] is the logarithm of the sum over s <= t of exp of the scores of the steps (before log_sum is subtracted), computed from the given queries, keys and log_gate.
All inputs are finite; a program needn't handle non-finite values.
Results may differ from a plain program's by a relative error of at most 0.005.
Values may be sent and summed in bfloat16 or wider, within the bound.
A program may use at most 64 MiB of HBM per device.

v0:
```python
import jax
import jax.numpy as jnp
from jax import lax
from jax.sharding import PartitionSpec as P

HDIM = 64
NEG_LARGE = -1e30


def prefix(x, axis, combine, identity):
    size, place = (lax.axis_size(axis), lax.axis_index(axis))
    everything = lax.all_gather(x, axis)
    start = jnp.broadcast_to(jnp.asarray(identity, x.dtype), x.shape)

    def hop(k, before):
        reached = k < place
        new = combine(before, everything[k])
        return jnp.where(reached, new, before)

    return lax.fori_loop(0, size, hop, start)


def shifted(x, axis, by):
    size = lax.axis_size(axis)
    pairs = [(i, i + by) for i in range(size) if 0 <= i + by < size]
    return lax.ppermute(x, axis, pairs)


def shifted_2(x, axis, by):
    size = lax.axis_size(axis)
    return lax.ppermute(x, axis, [(i, (i + by) % size) for i in range(size)])


def add_pair(earlier, later):
    return earlier + later


def body(queries, keys, values, log_gate, log_sum, output, cotangent, normed):
    tokens = queries.shape[0]
    head_count = log_gate.shape[0]
    kv_width = keys.shape[1]
    kv_heads = kv_width // HDIM
    groups = head_count // kv_heads
    inverse_root = HDIM ** (-0.5)
    devices = lax.axis_size("sp")
    my_index = lax.axis_index("sp")
    depth = 8
    totals = jnp.sum(log_gate, axis=1)
    before = prefix(totals, "sp", add_pair, jnp.zeros_like(totals))
    cumulative = jnp.cumsum(log_gate, axis=1) + before[:, None]
    row_terms = jnp.sum(
        (output.astype(jnp.float32) * cotangent.astype(jnp.float32)).reshape(
            tokens, head_count, HDIM
        ),
        axis=2,
    ).T
    query_split = queries.reshape(tokens, kv_heads, groups, HDIM)
    cotan_split = cotangent.reshape(tokens, kv_heads, groups, HDIM)
    cum_rows = cumulative.reshape(kv_heads, groups, tokens)
    lse_rows = log_sum.reshape(kv_heads, groups, tokens)
    term_rows = row_terms.reshape(kv_heads, groups, tokens)
    positions = my_index * tokens + jnp.arange(tokens)
    last_row = my_index * tokens + tokens - 1

    def visit_bundle(bundle, bundle_cum, key_pos):
        count = bundle.shape[0]
        block_rows = bundle.shape[1]
        key_rows = count * block_rows
        flat = bundle.reshape(key_rows, 2 * kv_width)
        flat_cum = jnp.transpose(bundle_cum, (1, 0, 2)).reshape(kv_heads, groups, key_rows)
        flat_pos = key_pos.reshape(key_rows)
        key_part = flat[:, :kv_width].reshape(key_rows, kv_heads, HDIM)
        value_part = flat[:, kv_width:].reshape(key_rows, kv_heads, HDIM)

        def attend(unused):
            scores = (
                jnp.einsum(
                    "qhgd,khd->hgqk", query_split, key_part, preferred_element_type=jnp.float32
                )
                * inverse_root
            )
            scores = (
                scores + cum_rows[:, :, :, None] - flat_cum[:, :, None, :] - lse_rows[:, :, :, None]
            )
            allowed = flat_pos[None, :] <= positions[:, None]
            weights = jnp.exp(jnp.where(allowed, scores, NEG_LARGE))
            upstream = jnp.einsum(
                "qhgd,khd->hgqk", cotan_split, value_part, preferred_element_type=jnp.float32
            )
            dscore_low = (weights * (upstream - term_rows[:, :, :, None])).astype(jnp.bfloat16)
            weights_low = weights.astype(jnp.bfloat16)
            query_add = (
                jnp.einsum(
                    "hgqk,khd->qhgd", dscore_low, key_part, preferred_element_type=jnp.float32
                )
                * inverse_root
            )
            key_add = (
                jnp.einsum(
                    "hgqk,qhgd->khd", dscore_low, query_split, preferred_element_type=jnp.float32
                )
                * inverse_root
            )
            value_add = jnp.einsum(
                "hgqk,qhgd->khd", weights_low, cotan_split, preferred_element_type=jnp.float32
            )
            joined = jnp.concatenate(
                [key_add.reshape(key_rows, kv_width), value_add.reshape(key_rows, kv_width)], axis=1
            )
            return (query_add, joined.reshape(count, block_rows, 2 * kv_width))

        def nothing(unused):
            return (
                jnp.zeros((tokens, kv_heads, groups, HDIM), jnp.float32),
                jnp.zeros((count, block_rows, 2 * kv_width), jnp.float32),
            )

        return lax.cond(jnp.min(flat_pos) <= last_row, attend, nothing, 0)

    stacked = jnp.concatenate([keys, values], axis=1)
    query_start = jnp.zeros((tokens, kv_heads, groups, HDIM), jnp.float32)
    copies = jnp.arange(depth)
    turns = devices // depth
    bundle_pieces = [stacked]
    bundle_cums = [cumulative]
    for step in range(1, depth):
        bundle_pieces.append(shifted(stacked, "sp", step))
        bundle_cums.append(shifted(cumulative, "sp", step))

    def turn(turn_index, state_now):
        query_total, bundle, bundle_cum, bundle_grads = state_now
        anchor = (my_index - depth * turn_index) % devices
        blocks = (anchor - copies) % devices
        key_pos = blocks[:, None] * tokens + jnp.arange(tokens)[None, :]
        query_add, grad_add = visit_bundle(bundle, bundle_cum, key_pos)
        bundle = shifted(bundle, "sp", depth)
        bundle_cum, bundle_grads = shifted_2((bundle_cum, bundle_grads + grad_add), "sp", depth)
        return (query_total + query_add, bundle, bundle_cum, bundle_grads)

    start_state = (
        query_start,
        jnp.stack(bundle_pieces),
        jnp.stack(bundle_cums),
        jnp.zeros((depth, tokens, 2 * kv_width), jnp.float32),
    )
    finished = lax.fori_loop(0, turns, turn, start_state)
    query_total = finished[0]
    final_grads = finished[3]
    gradients = final_grads[0]
    for step in range(1, depth):
        gradients = gradients + shifted(final_grads[step], "sp", -step)
    query_grad = query_total.reshape(tokens, head_count * HDIM).astype(jnp.bfloat16)
    key_grad = gradients[:, :kv_width].astype(jnp.bfloat16)
    value_grad = gradients[:, kv_width:].astype(jnp.bfloat16)
    whole_rows = lax.all_gather(normed, "tp", axis=1, tiled=True)
    weight_grad = lax.psum_scatter(
        lax.dot_general(
            whole_rows, key_grad, (((0,), (0,)), ((), ())), preferred_element_type=jnp.float32
        ),
        "sp",
        scatter_dimension=0,
        tiled=True,
    )
    return (query_grad, key_grad, value_grad, weight_grad)


def solution(mesh):
    in_specs = (
        P("sp", "tp"),
        P("sp", "tp"),
        P("sp", "tp"),
        P("tp", "sp"),
        P("tp", "sp"),
        P("sp", "tp"),
        P("sp", "tp"),
        P("sp", "tp"),
    )
    out_specs = (P("sp", "tp"), P("sp", "tp"), P("sp", "tp"), P("sp", "tp"))
    return jax.shard_map(body, mesh=mesh, in_specs=in_specs, out_specs=out_specs, check_vma=False)
```

profile of v0, /device:TPU:0, one launch (start us, length us, event | category | flops | bytes accessed | tf_op | source)
XLA Modules:
  0.0 176.8 jit_solution(9886937687388479770)
XLA Ops:
  11.2 23.1 %all-reduce = f32[32]{0:T(128)S(1)} all-reduce(f32[32]{0:T(128)S(1)} %dynamic-update-slice), channel_id=2, replica_groups=mesh['sp'=8,'tp'=4] {'sp'}, use_global_device_ids=true, to_apply=%add | all-reduce | flops 32 | bytes 256
  34.7 1.6 collective-permute-start.13
  36.4 1.3 collective-permute-start.12
  37.7 1.3 collective-permute-start.11
  39.0 1.3 collective-permute-start.10
  40.3 2.5 %collective-permute-start.7 = (f32[4,128]{1,0:T(4,128)S(1)}, f32[4,128]{1,0:T(4,128)S(1)}, u32[]{:S(2)}, u32[]{:S(2)}) collective-permute-start(f32[4,128]{1,0:T(4,128)S(1)} %broadcast_add_fusion.1), channel_id=1, source_target_pairs={{0,4},{4,8},{8,12},{12,16},{16,20},{20,24},{24,28},{1,5},{5,9},{9,... | collective-permute-start | bytes 6152 | tf_op jit(solution)/shard_map/ppermute | solution.py:26
  47.9 2.5 %collective-permute-start.8 = (f32[4,128]{1,0:T(4,128)S(1)}, f32[4,128]{1,0:T(4,128)S(1)}, u32[]{:S(2)}, u32[]{:S(2)}) collective-permute-start(f32[4,128]{1,0:T(4,128)S(1)} %broadcast_add_fusion.1), channel_id=1, source_target_pairs={{0,8},{4,12},{8,16},{12,20},{16,24},{20,28},{1,9},{5,13},{9,17},{1... | collective-permute-start | bytes 6152 | tf_op jit(solution)/shard_map/ppermute | solution.py:26
  50.4 1.3 collective-permute-done.8
  51.7 3.9 %collective-permute-start.9 = (f32[4,128]{1,0:T(4,128)S(1)}, f32[4,128]{1,0:T(4,128)S(1)}, u32[]{:S(2)}, u32[]{:S(2)}) collective-permute-start(f32[4,128]{1,0:T(4,128)S(1)} %broadcast_add_fusion.1), channel_id=1, source_target_pairs={{0,12},{4,16},{8,20},{12,24},{16,28},{1,13},{5,17},{9,21},{13,25},... | collective-permute-start | bytes 6152 | tf_op jit(solution)/shard_map/ppermute | solution.py:26
  55.6 1.3 collective-permute-done.9
  56.9 5.1 %collective-permute-start.5 = (bf16[128,128]{1,0:T(8,128)(2,1)S(1)}, bf16[128,128]{1,0:T(8,128)(2,1)S(1)}, u32[]{:S(2)}, u32[]{:S(2)}) collective-permute-start(bf16[128,128]{1,0:T(8,128)(2,1)S(1)} %get-tuple-element.251), channel_id=1, source_target_pairs={{0,24},{4,28},{1,25},{5,29},{2,26},{6,30},{3,27},{7,31}} | collective-permute-start | bytes 98312 | tf_op jit(solution)/shard_map/ppermute | solution.py:26
  62.0 1.3 collective-permute-start.4
  63.3 1.3 collective-permute-start.3
  64.6 1.6 collective-permute-start.2
  66.3 3.0 %collective-permute-start = (bf16[128,128]{1,0:T(8,128)(2,1)S(1)}, bf16[128,128]{1,0:T(8,128)(2,1)S(1)}, u32[]{:S(2)}, u32[]{:S(2)}) collective-permute-start(bf16[128,128]{1,0:T(8,128)(2,1)S(1)} %get-tuple-element.251), channel_id=1, source_target_pairs={{0,4},{4,8},{8,12},{12,16},{16,20},{20,24},{24,28},{1,5},{5,9},{9,... | collective-permute-start | bytes 98312 | tf_op jit(solution)/shard_map/ppermute | solution.py:26
  69.3 1.6 collective-permute-done
  70.9 4.2 %collective-permute-start.1 = (bf16[128,128]{1,0:T(8,128)(2,1)S(1)}, bf16[128,128]{1,0:T(8,128)(2,1)S(1)}, u32[]{:S(2)}, u32[]{:S(2)}) collective-permute-start(bf16[128,128]{1,0:T(8,128)(2,1)S(1)} %get-tuple-element.251), channel_id=1, source_target_pairs={{0,8},{4,12},{8,16},{12,20},{16,24},{20,28},{1,9},{5,13},{9,17},{1... | collective-permute-start | bytes 98312 | tf_op jit(solution)/shard_map/ppermute | solution.py:26
  75.1 1.6 collective-permute-done.1
  76.7 1.6 collective-permute-start.6
  78.4 1.5 collective-permute-done.6
  79.9 5.7 %conditional.1 = (f32[8,128,128]{1,2,0:T(8,128)S(1)}, bf16[128,256]{1,0:T(8,128)(2,1)S(1)}) conditional(s32[]{:T(128)} %convert_element_type.39, () %tuple.37, (s32[8,128]{1,0:T(8,128)S(1)}, s32[]{:T(128)}, s32[128]{0:T(128)S(1)}, bf16[8,128,128]{2,1,0:T(8,128)(2,1)S(1)}, bf16[128,256]{1,0:T(8,128)(2,1)}, /*index=5*/f32[4,128]{1,0:T(4,128)S(1)}, ...), branch_computations={%region_6.7_spmd, %region_7.8_spmd} | conditional | flops 340656256 | bytes 13856276 | solution.py:118
  82.1 1.5 fusion.21
  85.7 1.3 collective-permute-start.15
  87.0 1.3 collective-permute-start.21
  88.3 1.3 collective-permute-start.20
  89.6 1.3 collective-permute-start.19
  90.9 1.3 collective-permute-start.18
  92.2 1.3 collective-permute-start.17
  93.5 2.3 %collective-permute-done.21 = f32[128,128]{0,1:T(8,128)S(1)} collective-permute-done((f32[128,128]{0,1:T(8,128)S(1)}, f32[128,128]{0,1:T(8,128)S(1)}, u32[]{:S(2)}, u32[]{:S(2)}) %collective-permute-start.21) | collective-permute-done | bytes 65568 | tf_op jit(solution)/shard_map/ppermute | solution.py:26
  95.8 1.3 collective-permute-start.16
  97.1 7.2 %all_gather.11 = bf16[128,2048]{1,0:T(8,128)(2,1)S(1)} all-gather(bf16[128,512]{1,0:T(8,128)(2,1)S(1)} %copy-done), channel_id=1, replica_groups=mesh['sp'=8,'tp'=4] {'tp'}, dimensions={1}, use_global_device_ids=true | all-gather | bytes 655360 | tf_op jit(solution)/shard_map/all_gather | solution.py:155
  106.1 63.9 %reduce-scatter.2.cloned.1.call-done = f32[256,64]{0,1:T(8,128)} async-done(((f32[2048,64]{0,1:T(8,128)}), f32[256,64]{0,1:T(8,128)}) %reduce-scatter.2.cloned.1.call-update) | async-done | bytes 65552 | tf_op jit(solution)/shard_map/reduce_scatter | solution.py:156
  (82 shorter events, 14.4 us)
Async XLA Ops:
  7.2 162.8 %reduce-scatter.2.cloned.1.call-start = ((), (), s32[]{:S(2)}) async-start(), calls=%async_computation.1 | async-start | bytes 589824 | tf_op jit(solution)/shard_map/reduce_scatter | solution.py:156
  34.7 31.6 %collective-permute-start.13 = (f32[4,128]{1,0:T(4,128)S(1)}, f32[4,128]{1,0:T(4,128)S(1)}, u32[]{:S(2)}, u32[]{:S(2)}) collective-permute-start(f32[4,128]{1,0:T(4,128)S(1)} %broadcast_add_fusion.1), channel_id=1, source_target_pairs={{0,28},{1,29},{2,30},{3,31}} | collective-permute-start | bytes 6152 | tf_op jit(solution)/shard_map/ppermute | solution.py:26
  36.4 28.2 %collective-permute-start.12 = (f32[4,128]{1,0:T(4,128)S(1)}, f32[4,128]{1,0:T(4,128)S(1)}, u32[]{:S(2)}, u32[]{:S(2)}) collective-permute-start(f32[4,128]{1,0:T(4,128)S(1)} %broadcast_add_fusion.1), channel_id=1, source_target_pairs={{0,24},{4,28},{1,25},{5,29},{2,26},{6,30},{3,27},{7,31}} | collective-permute-start | bytes 6152 | tf_op jit(solution)/shard_map/ppermute | solution.py:26
  37.7 25.6 %collective-permute-start.11 = (f32[4,128]{1,0:T(4,128)S(1)}, f32[4,128]{1,0:T(4,128)S(1)}, u32[]{:S(2)}, u32[]{:S(2)}) collective-permute-start(f32[4,128]{1,0:T(4,128)S(1)} %broadcast_add_fusion.1), channel_id=1, source_target_pairs={{0,20},{4,24},{8,28},{1,21},{5,25},{9,29},{2,22},{6,26},{10,30},{3... | collective-permute-start | bytes 6152 | tf_op jit(solution)/shard_map/ppermute | solution.py:26
  39.0 23.0 %collective-permute-start.10 = (f32[4,128]{1,0:T(4,128)S(1)}, f32[4,128]{1,0:T(4,128)S(1)}, u32[]{:S(2)}, u32[]{:S(2)}) collective-permute-start(f32[4,128]{1,0:T(4,128)S(1)} %broadcast_add_fusion.1), channel_id=1, source_target_pairs={{0,16},{4,20},{8,24},{12,28},{1,17},{5,21},{9,25},{13,29},{2,18},{... | collective-permute-start | bytes 6152 | tf_op jit(solution)/shard_map/ppermute | solution.py:26
  40.3 7.6 %collective-permute-start.7 = (f32[4,128]{1,0:T(4,128)S(1)}, f32[4,128]{1,0:T(4,128)S(1)}, u32[]{:S(2)}, u32[]{:S(2)}) collective-permute-start(f32[4,128]{1,0:T(4,128)S(1)} %broadcast_add_fusion.1), channel_id=1, source_target_pairs={{0,4},{4,8},{8,12},{12,16},{16,20},{20,24},{24,28},{1,5},{5,9},{9,... | collective-permute-start | bytes 6152 | tf_op jit(solution)/shard_map/ppermute | solution.py:26
  47.9 3.8 %collective-permute-start.8 = (f32[4,128]{1,0:T(4,128)S(1)}, f32[4,128]{1,0:T(4,128)S(1)}, u32[]{:S(2)}, u32[]{:S(2)}) collective-permute-start(f32[4,128]{1,0:T(4,128)S(1)} %broadcast_add_fusion.1), channel_id=1, source_target_pairs={{0,8},{4,12},{8,16},{12,20},{16,24},{20,28},{1,9},{5,13},{9,17},{1... | collective-permute-start | bytes 6152 | tf_op jit(solution)/shard_map/ppermute | solution.py:26
  51.7 5.2 %collective-permute-start.9 = (f32[4,128]{1,0:T(4,128)S(1)}, f32[4,128]{1,0:T(4,128)S(1)}, u32[]{:S(2)}, u32[]{:S(2)}) collective-permute-start(f32[4,128]{1,0:T(4,128)S(1)} %broadcast_add_fusion.1), channel_id=1, source_target_pairs={{0,12},{4,16},{8,20},{12,24},{16,28},{1,13},{5,17},{9,21},{13,25},... | collective-permute-start | bytes 6152 | tf_op jit(solution)/shard_map/ppermute | solution.py:26
  56.9 21.5 %collective-permute-start.5 = (bf16[128,128]{1,0:T(8,128)(2,1)S(1)}, bf16[128,128]{1,0:T(8,128)(2,1)S(1)}, u32[]{:S(2)}, u32[]{:S(2)}) collective-permute-start(bf16[128,128]{1,0:T(8,128)(2,1)S(1)} %get-tuple-element.251), channel_id=1, source_target_pairs={{0,24},{4,28},{1,25},{5,29},{2,26},{6,30},{3,27},{7,31}} | collective-permute-start | bytes 98312 | tf_op jit(solution)/shard_map/ppermute | solution.py:26
  62.0 16.4 %collective-permute-start.4 = (bf16[128,128]{1,0:T(8,128)(2,1)S(1)}, bf16[128,128]{1,0:T(8,128)(2,1)S(1)}, u32[]{:S(2)}, u32[]{:S(2)}) collective-permute-start(bf16[128,128]{1,0:T(8,128)(2,1)S(1)} %get-tuple-element.251), channel_id=1, source_target_pairs={{0,20},{4,24},{8,28},{1,21},{5,25},{9,29},{2,22},{6,26},{10,30},{3... | collective-permute-start | bytes 98312 | tf_op jit(solution)/shard_map/ppermute | solution.py:26
  63.3 15.0 %collective-permute-start.3 = (bf16[128,128]{1,0:T(8,128)(2,1)S(1)}, bf16[128,128]{1,0:T(8,128)(2,1)S(1)}, u32[]{:S(2)}, u32[]{:S(2)}) collective-permute-start(bf16[128,128]{1,0:T(8,128)(2,1)S(1)} %get-tuple-element.251), channel_id=1, source_target_pairs={{0,16},{4,20},{8,24},{12,28},{1,17},{5,21},{9,25},{13,29},{2,18},{... | collective-permute-start | bytes 98312 | tf_op jit(solution)/shard_map/ppermute | solution.py:26
  64.6 13.7 %collective-permute-start.2 = (bf16[128,128]{1,0:T(8,128)(2,1)S(1)}, bf16[128,128]{1,0:T(8,128)(2,1)S(1)}, u32[]{:S(2)}, u32[]{:S(2)}) collective-permute-start(bf16[128,128]{1,0:T(8,128)(2,1)S(1)} %get-tuple-element.251), channel_id=1, source_target_pairs={{0,12},{4,16},{8,20},{12,24},{16,28},{1,13},{5,17},{9,21},{13,25},... | collective-permute-start | bytes 98312 | tf_op jit(solution)/shard_map/ppermute | solution.py:26
  66.3 4.6 %collective-permute-start = (bf16[128,128]{1,0:T(8,128)(2,1)S(1)}, bf16[128,128]{1,0:T(8,128)(2,1)S(1)}, u32[]{:S(2)}, u32[]{:S(2)}) collective-permute-start(bf16[128,128]{1,0:T(8,128)(2,1)S(1)} %get-tuple-element.251), channel_id=1, source_target_pairs={{0,4},{4,8},{8,12},{12,16},{16,20},{20,24},{24,28},{1,5},{5,9},{9,... | collective-permute-start | bytes 98312 | tf_op jit(solution)/shard_map/ppermute | solution.py:26
  70.9 5.8 %collective-permute-start.1 = (bf16[128,128]{1,0:T(8,128)(2,1)S(1)}, bf16[128,128]{1,0:T(8,128)(2,1)S(1)}, u32[]{:S(2)}, u32[]{:S(2)}) collective-permute-start(bf16[128,128]{1,0:T(8,128)(2,1)S(1)} %get-tuple-element.251), channel_id=1, source_target_pairs={{0,8},{4,12},{8,16},{12,20},{16,24},{20,28},{1,9},{5,13},{9,17},{1... | collective-permute-start | bytes 98312 | tf_op jit(solution)/shard_map/ppermute | solution.py:26
  76.7 3.2 %collective-permute-start.6 = (bf16[128,128]{1,0:T(8,128)(2,1)S(1)}, bf16[128,128]{1,0:T(8,128)(2,1)S(1)}, u32[]{:S(2)}, u32[]{:S(2)}) collective-permute-start(bf16[128,128]{1,0:T(8,128)(2,1)S(1)} %get-tuple-element.251), channel_id=1, source_target_pairs={{0,28},{1,29},{2,30},{3,31}} | collective-permute-start | bytes 98312 | tf_op jit(solution)/shard_map/ppermute | solution.py:26
  79.9 17.2 %copy-start = (bf16[128,512]{1,0:T(8,128)(2,1)S(1)}, bf16[128,512]{1,0:T(8,128)(2,1)}, u32[]{:S(2)}) copy-start(bf16[128,512]{1,0:T(8,128)(2,1)} %param.19) | copy-start | bytes 393220
  85.5 84.4 %copy-start.2 = (bf16[128,256]{1,0:T(8,128)(2,1)}, bf16[128,256]{1,0:T(8,128)(2,1)S(1)}, u32[]{:S(2)}) copy-start(bf16[128,256]{1,0:T(8,128)(2,1)S(1)} %get-tuple-element.241) | copy-start | bytes 196612
  85.7 6.5 %collective-permute-start.15 = (f32[128,128]{0,1:T(8,128)S(1)}, f32[128,128]{0,1:T(8,128)S(1)}, u32[]{:S(2)}, u32[]{:S(2)}) collective-permute-start(f32[128,128]{0,1:T(8,128)S(1)} %get-tuple-element.254), channel_id=1, source_target_pairs={{4,0},{8,4},{12,8},{16,12},{20,16},{24,20},{28,24},{5,1},{9,5},{13... | collective-permute-start | bytes 196616 | tf_op jit(solution)/shard_map/ppermute | solution.py:26
  87.0 8.9 %collective-permute-start.21 = (f32[128,128]{0,1:T(8,128)S(1)}, f32[128,128]{0,1:T(8,128)S(1)}, u32[]{:S(2)}, u32[]{:S(2)}) collective-permute-start(f32[128,128]{0,1:T(8,128)S(1)} %get-tuple-element.255), channel_id=1, source_target_pairs={{28,0},{29,1},{30,2},{31,3}} | collective-permute-start | bytes 196616 | tf_op jit(solution)/shard_map/ppermute | solution.py:26
  88.3 16.1 %collective-permute-start.20 = (f32[128,128]{0,1:T(8,128)S(1)}, f32[128,128]{0,1:T(8,128)S(1)}, u32[]{:S(2)}, u32[]{:S(2)}) collective-permute-start(f32[128,128]{0,1:T(8,128)S(1)} %get-tuple-element.256), channel_id=1, source_target_pairs={{24,0},{28,4},{25,1},{29,5},{26,2},{30,6},{27,3},{31,7}} | collective-permute-start | bytes 196616 | tf_op jit(solution)/shard_map/ppermute | solution.py:26
  89.6 14.8 %collective-permute-start.19 = (f32[128,128]{0,1:T(8,128)S(1)}, f32[128,128]{0,1:T(8,128)S(1)}, u32[]{:S(2)}, u32[]{:S(2)}) collective-permute-start(f32[128,128]{0,1:T(8,128)S(1)} %get-tuple-element.257), channel_id=1, source_target_pairs={{20,0},{24,4},{28,8},{21,1},{25,5},{29,9},{22,2},{26,6},{30,10},{2... | collective-permute-start | bytes 196616 | tf_op jit(solution)/shard_map/ppermute | solution.py:26
  90.9 13.5 %collective-permute-start.18 = (f32[128,128]{0,1:T(8,128)S(1)}, f32[128,128]{0,1:T(8,128)S(1)}, u32[]{:S(2)}, u32[]{:S(2)}) collective-permute-start(f32[128,128]{0,1:T(8,128)S(1)} %get-tuple-element.258), channel_id=1, source_target_pairs={{16,0},{20,4},{24,8},{28,12},{17,1},{21,5},{25,9},{29,13},{18,2},{... | collective-permute-start | bytes 196616 | tf_op jit(solution)/shard_map/ppermute | solution.py:26
  92.2 12.2 %collective-permute-start.17 = (f32[128,128]{0,1:T(8,128)S(1)}, f32[128,128]{0,1:T(8,128)S(1)}, u32[]{:S(2)}, u32[]{:S(2)}) collective-permute-start(f32[128,128]{0,1:T(8,128)S(1)} %get-tuple-element.259), channel_id=1, source_target_pairs={{12,0},{16,4},{20,8},{24,12},{28,16},{13,1},{17,5},{21,9},{25,13},... | collective-permute-start | bytes 196616 | tf_op jit(solution)/shard_map/ppermute | solution.py:26
  95.8 8.5 %collective-permute-start.16 = (f32[128,128]{0,1:T(8,128)S(1)}, f32[128,128]{0,1:T(8,128)S(1)}, u32[]{:S(2)}, u32[]{:S(2)}) collective-permute-start(f32[128,128]{0,1:T(8,128)S(1)} %get-tuple-element.260), channel_id=1, source_target_pairs={{8,0},{12,4},{16,8},{20,12},{24,16},{28,20},{9,1},{13,5},{17,9},{2... | collective-permute-start | bytes 196616 | tf_op jit(solution)/shard_map/ppermute | solution.py:26
  105.0 65.0 %copy-start.1 = (bf16[128,64]{0,1:T(8,128)(2,1)}, bf16[128,64]{0,1:T(8,128)(2,1)S(1)}, u32[]{:S(2)}) copy-start(bf16[128,64]{0,1:T(8,128)(2,1)S(1)} %get-tuple-element.262) | copy-start | bytes 49156
  (1 other events, 0.0 us)
Sparse Core Ops, SparseCore 0:
  106.2 63.7 reduce-scatter.1
where the time goes:
time: 178 us; the launch traced here: 177 us
  waiting for transfers between devices  73.4 us (41%)
  starting transfers between devices  41.6 us (23%)
  blocking collectives  30.3 us (17%)
  between operations  15.8 us (9%)
  local copies, waits for them, and re-layouts  8.07 us (5%)
  matrix products  4.19 us (2%)
  other arithmetic  3.18 us (2%)
    reduce_scatter x1, waiting for transfers between devices, body(): lax.psum_scatter(lax.dot_general(whole_rows, key_grad, (((0,), (0,)), (()...  63.9 us
    ppermute x21, starting transfers between devices, shifted(): return lax.ppermute(x, axis, pairs)  41.5 us
    unnamed x1, blocking collectives  23.1 us
    ppermute x21, waiting for transfers between devices, shifted(): return lax.ppermute(x, axis, pairs)  9.53 us
    all_gather x1, blocking collectives, body(): whole_rows = lax.all_gather(normed, 'tp', axis=1, tiled=True)  7.21 us
    unnamed x25, local copies, waits for them, and re-layouts  5.18 us
  transfers between devices with their start and end apart: 23, of which 7 were waited for; matrix products, arithmetic and copies ran while one was open for 3% of the time, Pallas kernels for 0%

commit v1 on v0

--- a/solution.py
+++ b/solution.py
@@ -152,7 +152,9 @@
     query_grad = query_total.reshape(tokens, head_count * HDIM).astype(jnp.bfloat16)
     key_grad = gradients[:, :kv_width].astype(jnp.bfloat16)
     value_grad = gradients[:, kv_width:].astype(jnp.bfloat16)
-    whole_rows = lax.all_gather(normed, "tp", axis=1, tiled=True)
+    whole_rows = jnp.concatenate(
+        lax.all_to_all(jnp.stack([normed] * lax.axis_size("tp")), "tp", 0, 0), axis=1
+    )
     weight_grad = lax.psum_scatter(
         lax.dot_general(
             whole_rows, key_grad, (((0,), (0,)), ((), ())), preferred_element_type=jnp.float32

time: 178 us -> 206 us (1.16)
  starting transfers between devices: 41.6 us -> 69.2 us
  blocking collectives: 30.3 us -> 17.9 us
  waiting for transfers between devices: 73.4 us -> 84.6 us
    ppermute x21, starting transfers between devices: 41.5 us -> 64.6 us  [shifted(): return lax.ppermute(x, axis, pairs)]
    all_to_all x0 -> x1, waiting for transfers between devices: none -> 8.03 us  [body(): lax.all_to_all(jnp.stack([normed] * lax.axis_size('tp')), 'tp', 0, 0)]
    all_gather x1 -> x0, blocking collectives: 7.21 us -> none  [body(): whole_rows = lax.all_gather(normed, 'tp', axis=1, tiled=True)]
    unnamed x1, blocking collectives: 23.1 us -> 17.9 us
    all_to_all x0 -> x1, starting transfers between devices: none -> 3.47 us  [body(): lax.all_to_all(jnp.stack([normed] * lax.axis_size('tp')), 'tp', 0, 0)]
    unnamed x25 -> x24, local copies, waits for them, and re-layouts: 5.18 us -> 6.19 us
  transfers between devices with their start and end apart: 23 -> 24, of which waited for: 7 -> 10; matrix products, arithmetic and copies ran while one was open for 3% -> 4% of each run, Pallas kernels for 0% -> 0%
where the time goes in v1:
time: 206 us; the launch traced here: 205 us
  waiting for transfers between devices  84.6 us (41%)
  starting transfers between devices  69.2 us (34%)
  blocking collectives  17.9 us (9%)
  between operations  15.8 us (8%)
  local copies, waits for them, and re-layouts  9.1 us (4%)
  matrix products  4.35 us (2%)
  other arithmetic  3.99 us (2%)
    reduce_scatter x1, waiting for transfers between devices, body(): lax.psum_scatter(lax.dot_general(whole_rows, key_grad, (((0,), (0,)), (()...  65 us
    ppermute x21, starting transfers between devices, shifted(): return lax.ppermute(x, axis, pairs)  64.6 us
    unnamed x1, blocking collectives  17.9 us
    ppermute x21, waiting for transfers between devices, shifted(): return lax.ppermute(x, axis, pairs)  11.5 us
    all_to_all x1, waiting for transfers between devices, body(): lax.all_to_all(jnp.stack([normed] * lax.axis_size('tp')), 'tp', 0, 0)  8.03 us
    unnamed x24, local copies, waits for them, and re-layouts  6.19 us
  transfers between devices with their start and end apart: 24, of which 10 were waited for; matrix products, arithmetic and copies ran while one was open for 4% of the time, Pallas kernels for 0%

profile of v1, /device:TPU:0, one launch (start us, length us, event | category | flops | bytes accessed | tf_op | source)
XLA Modules:
  0.0 205.2 jit_solution(13457727629967190589)
XLA Ops:
  8.9 4.9 %collective-permute-start = (bf16[128,128]{1,0:T(8,128)(2,1)S(1)}, bf16[128,128]{1,0:T(8,128)(2,1)S(1)}, u32[]{:S(2)}, u32[]{:S(2)}) collective-permute-start(bf16[128,128]{1,0:T(8,128)(2,1)S(1)} %get-tuple-element.251), channel_id=1, source_target_pairs={{0,4},{4,8},{8,12},{12,16},{16,20},{20,24},{24,28},{1,5},{5,9},{9,... | collective-permute-start | bytes 98312 | tf_op jit(solution)/shard_map/ppermute | solution.py:26
  13.8 3.5 %collective-permute-start.1 = (bf16[128,128]{1,0:T(8,128)(2,1)S(1)}, bf16[128,128]{1,0:T(8,128)(2,1)S(1)}, u32[]{:S(2)}, u32[]{:S(2)}) collective-permute-start(bf16[128,128]{1,0:T(8,128)(2,1)S(1)} %get-tuple-element.251), channel_id=1, source_target_pairs={{0,8},{4,12},{8,16},{12,20},{16,24},{20,28},{1,9},{5,13},{9,17},{1... | collective-permute-start | bytes 98312 | tf_op jit(solution)/shard_map/ppermute | solution.py:26
  17.3 4.5 %collective-permute-start.2 = (bf16[128,128]{1,0:T(8,128)(2,1)S(1)}, bf16[128,128]{1,0:T(8,128)(2,1)S(1)}, u32[]{:S(2)}, u32[]{:S(2)}) collective-permute-start(bf16[128,128]{1,0:T(8,128)(2,1)S(1)} %get-tuple-element.251), channel_id=1, source_target_pairs={{0,12},{4,16},{8,20},{12,24},{16,28},{1,13},{5,17},{9,21},{13,25},... | collective-permute-start | bytes 98312 | tf_op jit(solution)/shard_map/ppermute | solution.py:26
  21.8 1.9 collective-permute-start.3
  27.7 17.9 %all-reduce = f32[32]{0:T(128)S(1)} all-reduce(f32[32]{0:T(128)S(1)} %dynamic-update-slice), channel_id=2, replica_groups=mesh['sp'=8,'tp'=4] {'sp'}, use_global_device_ids=true, to_apply=%add | all-reduce | flops 32 | bytes 256
  46.1 3.1 %collective-permute-start.7 = (f32[4,128]{1,0:T(4,128)S(1)}, f32[4,128]{1,0:T(4,128)S(1)}, u32[]{:S(2)}, u32[]{:S(2)}) collective-permute-start(f32[4,128]{1,0:T(4,128)S(1)} %broadcast_add_fusion.1), channel_id=1, source_target_pairs={{0,4},{4,8},{8,12},{12,16},{16,20},{20,24},{24,28},{1,5},{5,9},{9,... | collective-permute-start | bytes 6152 | tf_op jit(solution)/shard_map/ppermute | solution.py:26
  52.6 1.5 collective-permute-start.8
  55.4 3.5 %collective-permute-start.9 = (f32[4,128]{1,0:T(4,128)S(1)}, f32[4,128]{1,0:T(4,128)S(1)}, u32[]{:S(2)}, u32[]{:S(2)}) collective-permute-start(f32[4,128]{1,0:T(4,128)S(1)} %broadcast_add_fusion.1), channel_id=1, source_target_pairs={{0,12},{4,16},{8,20},{12,24},{16,28},{1,13},{5,17},{9,21},{13,25},... | collective-permute-start | bytes 6152 | tf_op jit(solution)/shard_map/ppermute | solution.py:26
  60.2 6.0 %collective-permute-start.10 = (f32[4,128]{1,0:T(4,128)S(1)}, f32[4,128]{1,0:T(4,128)S(1)}, u32[]{:S(2)}, u32[]{:S(2)}) collective-permute-start(f32[4,128]{1,0:T(4,128)S(1)} %broadcast_add_fusion.1), channel_id=1, source_target_pairs={{0,16},{4,20},{8,24},{12,28},{1,17},{5,21},{9,25},{13,29},{2,18},{... | collective-permute-start | bytes 6152 | tf_op jit(solution)/shard_map/ppermute | solution.py:26
  67.5 4.9 %collective-permute-start.11 = (f32[4,128]{1,0:T(4,128)S(1)}, f32[4,128]{1,0:T(4,128)S(1)}, u32[]{:S(2)}, u32[]{:S(2)}) collective-permute-start(f32[4,128]{1,0:T(4,128)S(1)} %broadcast_add_fusion.1), channel_id=1, source_target_pairs={{0,20},{4,24},{8,28},{1,21},{5,25},{9,29},{2,22},{6,26},{10,30},{3... | collective-permute-start | bytes 6152 | tf_op jit(solution)/shard_map/ppermute | solution.py:26
  72.4 1.3 collective-permute-done.11
  73.7 8.6 %collective-permute-start.12 = (f32[4,128]{1,0:T(4,128)S(1)}, f32[4,128]{1,0:T(4,128)S(1)}, u32[]{:S(2)}, u32[]{:S(2)}) collective-permute-start(f32[4,128]{1,0:T(4,128)S(1)} %broadcast_add_fusion.1), channel_id=1, source_target_pairs={{0,24},{4,28},{1,25},{5,29},{2,26},{6,30},{3,27},{7,31}} | collective-permute-start | bytes 6152 | tf_op jit(solution)/shard_map/ppermute | solution.py:26
  82.3 1.3 collective-permute-done.12
  83.6 3.7 %collective-permute-start.13 = (f32[4,128]{1,0:T(4,128)S(1)}, f32[4,128]{1,0:T(4,128)S(1)}, u32[]{:S(2)}, u32[]{:S(2)}) collective-permute-start(f32[4,128]{1,0:T(4,128)S(1)} %broadcast_add_fusion.1), channel_id=1, source_target_pairs={{0,28},{1,29},{2,30},{3,31}} | collective-permute-start | bytes 6152 | tf_op jit(solution)/shard_map/ppermute | solution.py:26
  87.4 1.3 collective-permute-done.13
  88.6 1.3 collective-permute-start.4
  90.0 1.6 collective-permute-start.5
  91.6 6.5 %collective-permute-start.6 = (bf16[128,128]{1,0:T(8,128)(2,1)S(1)}, bf16[128,128]{1,0:T(8,128)(2,1)S(1)}, u32[]{:S(2)}, u32[]{:S(2)}) collective-permute-start(bf16[128,128]{1,0:T(8,128)(2,1)S(1)} %get-tuple-element.251), channel_id=1, source_target_pairs={{0,28},{1,29},{2,30},{3,31}} | collective-permute-start | bytes 98312 | tf_op jit(solution)/shard_map/ppermute | solution.py:26
  98.3 1.5 collective-permute-done.6
  99.8 5.7 %conditional.1 = (f32[8,128,128]{1,2,0:T(8,128)}, bf16[128,256]{1,0:T(8,128)(2,1)S(1)}) conditional(s32[]{:T(128)} %convert_element_type.39, () %tuple.37, (s32[8,128]{1,0:T(8,128)S(1)}, s32[]{:T(128)}, s32[128]{0:T(128)S(1)}, bf16[8,128,128]{2,1,0:T(8,128)(2,1)S(1)}, bf16[128,256]{1,0:T(8,128)(2,1)}, /*index=5*/f32[4,128]{1,0:T(4,128)S(1)}, ...), branch_computations={%region_6.7_spmd, %region_7.8_spmd} | conditional | flops 340656256 | bytes 14708356 | solution.py:118
  101.0 1.6 fusion.21
  106.6 1.3 collective-permute-start.21
  107.9 1.3 collective-permute-start.20
  109.2 1.3 collective-permute-start.19
  110.5 1.3 collective-permute-start.18
  111.8 1.3 collective-permute-start.17
  113.1 2.4 %collective-permute-done.21 = f32[128,128]{0,1:T(8,128)S(1)} collective-permute-done((f32[128,128]{0,1:T(8,128)S(1)}, f32[128,128]{0,1:T(8,128)S(1)}, u32[]{:S(2)}, u32[]{:S(2)}) %collective-permute-start.21) | collective-permute-done | bytes 65568 | tf_op jit(solution)/shard_map/ppermute | solution.py:26
  115.5 1.3 collective-permute-start.16
  116.8 1.3 collective-permute-start.15
  120.0 3.5 %all-to-all-start = ((bf16[4,128,512]{1,2,0:T(8,128)(2,1)}), bf16[4,128,512]{1,2,0:T(8,128)(2,1)S(1)}, u32[]{:S(2)}, u32[]{:S(2)}) async-start(bf16[4,128,512]{1,2,0:T(8,128)(2,1)} %stack.76), calls=%async_computation | async-start | bytes 1048576 | tf_op jit(solution)/shard_map/all_to_all | solution.py:156
  124.2 8.0 %all-to-all-done = bf16[4,128,512]{1,2,0:T(8,128)(2,1)S(1)} async-done(((bf16[4,128,512]{1,2,0:T(8,128)(2,1)}), bf16[4,128,512]{1,2,0:T(8,128)(2,1)S(1)}, u32[]{:S(2)}, u32[]{:S(2)}) %all-to-all-start) | async-done | bytes 524320 | tf_op jit(solution)/shard_map/all_to_all | solution.py:156
  133.4 65.0 %reduce-scatter.2.cloned.1.call-done = f32[256,64]{0,1:T(8,128)} async-done(((f32[2048,64]{0,1:T(8,128)}), f32[256,64]{0,1:T(8,128)}) %reduce-scatter.2.cloned.1.call-update) | async-done | bytes 65552 | tf_op jit(solution)/shard_map/reduce_scatter | solution.py:158
  (91 shorter events, 21.2 us)
Async XLA Ops:
  8.9 81.0 %collective-permute-start = (bf16[128,128]{1,0:T(8,128)(2,1)S(1)}, bf16[128,128]{1,0:T(8,128)(2,1)S(1)}, u32[]{:S(2)}, u32[]{:S(2)}) collective-permute-start(bf16[128,128]{1,0:T(8,128)(2,1)S(1)} %get-tuple-element.251), channel_id=1, source_target_pairs={{0,4},{4,8},{8,12},{12,16},{16,20},{20,24},{24,28},{1,5},{5,9},{9,... | collective-permute-start | bytes 98312 | tf_op jit(solution)/shard_map/ppermute | solution.py:26
  13.8 77.8 %collective-permute-start.1 = (bf16[128,128]{1,0:T(8,128)(2,1)S(1)}, bf16[128,128]{1,0:T(8,128)(2,1)S(1)}, u32[]{:S(2)}, u32[]{:S(2)}) collective-permute-start(bf16[128,128]{1,0:T(8,128)(2,1)S(1)} %get-tuple-element.251), channel_id=1, source_target_pairs={{0,8},{4,12},{8,16},{12,20},{16,24},{20,28},{1,9},{5,13},{9,17},{1... | collective-permute-start | bytes 98312 | tf_op jit(solution)/shard_map/ppermute | solution.py:26
  17.3 80.9 %collective-permute-start.2 = (bf16[128,128]{1,0:T(8,128)(2,1)S(1)}, bf16[128,128]{1,0:T(8,128)(2,1)S(1)}, u32[]{:S(2)}, u32[]{:S(2)}) collective-permute-start(bf16[128,128]{1,0:T(8,128)(2,1)S(1)} %get-tuple-element.251), channel_id=1, source_target_pairs={{0,12},{4,16},{8,20},{12,24},{16,28},{1,13},{5,17},{9,21},{13,25},... | collective-permute-start | bytes 98312 | tf_op jit(solution)/shard_map/ppermute | solution.py:26
  21.8 76.4 %collective-permute-start.3 = (bf16[128,128]{1,0:T(8,128)(2,1)S(1)}, bf16[128,128]{1,0:T(8,128)(2,1)S(1)}, u32[]{:S(2)}, u32[]{:S(2)}) collective-permute-start(bf16[128,128]{1,0:T(8,128)(2,1)S(1)} %get-tuple-element.251), channel_id=1, source_target_pairs={{0,16},{4,20},{8,24},{12,28},{1,17},{5,21},{9,25},{13,29},{2,18},{... | collective-permute-start | bytes 98312 | tf_op jit(solution)/shard_map/ppermute | solution.py:26
  46.1 6.5 %collective-permute-start.7 = (f32[4,128]{1,0:T(4,128)S(1)}, f32[4,128]{1,0:T(4,128)S(1)}, u32[]{:S(2)}, u32[]{:S(2)}) collective-permute-start(f32[4,128]{1,0:T(4,128)S(1)} %broadcast_add_fusion.1), channel_id=1, source_target_pairs={{0,4},{4,8},{8,12},{12,16},{16,20},{20,24},{24,28},{1,5},{5,9},{9,... | collective-permute-start | bytes 6152 | tf_op jit(solution)/shard_map/ppermute | solution.py:26
  52.6 2.8 %collective-permute-start.8 = (f32[4,128]{1,0:T(4,128)S(1)}, f32[4,128]{1,0:T(4,128)S(1)}, u32[]{:S(2)}, u32[]{:S(2)}) collective-permute-start(f32[4,128]{1,0:T(4,128)S(1)} %broadcast_add_fusion.1), channel_id=1, source_target_pairs={{0,8},{4,12},{8,16},{12,20},{16,24},{20,28},{1,9},{5,13},{9,17},{1... | collective-permute-start | bytes 6152 | tf_op jit(solution)/shard_map/ppermute | solution.py:26
  55.4 4.8 %collective-permute-start.9 = (f32[4,128]{1,0:T(4,128)S(1)}, f32[4,128]{1,0:T(4,128)S(1)}, u32[]{:S(2)}, u32[]{:S(2)}) collective-permute-start(f32[4,128]{1,0:T(4,128)S(1)} %broadcast_add_fusion.1), channel_id=1, source_target_pairs={{0,12},{4,16},{8,20},{12,24},{16,28},{1,13},{5,17},{9,21},{13,25},... | collective-permute-start | bytes 6152 | tf_op jit(solution)/shard_map/ppermute | solution.py:26
  60.2 7.3 %collective-permute-start.10 = (f32[4,128]{1,0:T(4,128)S(1)}, f32[4,128]{1,0:T(4,128)S(1)}, u32[]{:S(2)}, u32[]{:S(2)}) collective-permute-start(f32[4,128]{1,0:T(4,128)S(1)} %broadcast_add_fusion.1), channel_id=1, source_target_pairs={{0,16},{4,20},{8,24},{12,28},{1,17},{5,21},{9,25},{13,29},{2,18},{... | collective-permute-start | bytes 6152 | tf_op jit(solution)/shard_map/ppermute | solution.py:26
  67.5 6.2 %collective-permute-start.11 = (f32[4,128]{1,0:T(4,128)S(1)}, f32[4,128]{1,0:T(4,128)S(1)}, u32[]{:S(2)}, u32[]{:S(2)}) collective-permute-start(f32[4,128]{1,0:T(4,128)S(1)} %broadcast_add_fusion.1), channel_id=1, source_target_pairs={{0,20},{4,24},{8,28},{1,21},{5,25},{9,29},{2,22},{6,26},{10,30},{3... | collective-permute-start | bytes 6152 | tf_op jit(solution)/shard_map/ppermute | solution.py:26
  73.7 9.9 %collective-permute-start.12 = (f32[4,128]{1,0:T(4,128)S(1)}, f32[4,128]{1,0:T(4,128)S(1)}, u32[]{:S(2)}, u32[]{:S(2)}) collective-permute-start(f32[4,128]{1,0:T(4,128)S(1)} %broadcast_add_fusion.1), channel_id=1, source_target_pairs={{0,24},{4,28},{1,25},{5,29},{2,26},{6,30},{3,27},{7,31}} | collective-permute-start | bytes 6152 | tf_op jit(solution)/shard_map/ppermute | solution.py:26
  83.6 5.0 %collective-permute-start.13 = (f32[4,128]{1,0:T(4,128)S(1)}, f32[4,128]{1,0:T(4,128)S(1)}, u32[]{:S(2)}, u32[]{:S(2)}) collective-permute-start(f32[4,128]{1,0:T(4,128)S(1)} %broadcast_add_fusion.1), channel_id=1, source_target_pairs={{0,28},{1,29},{2,30},{3,31}} | collective-permute-start | bytes 6152 | tf_op jit(solution)/shard_map/ppermute | solution.py:26
  88.6 9.6 %collective-permute-start.4 = (bf16[128,128]{1,0:T(8,128)(2,1)S(1)}, bf16[128,128]{1,0:T(8,128)(2,1)S(1)}, u32[]{:S(2)}, u32[]{:S(2)}) collective-permute-start(bf16[128,128]{1,0:T(8,128)(2,1)S(1)} %get-tuple-element.251), channel_id=1, source_target_pairs={{0,20},{4,24},{8,28},{1,21},{5,25},{9,29},{2,22},{6,26},{10,30},{3... | collective-permute-start | bytes 98312 | tf_op jit(solution)/shard_map/ppermute | solution.py:26
  90.0 8.3 %collective-permute-start.5 = (bf16[128,128]{1,0:T(8,128)(2,1)S(1)}, bf16[128,128]{1,0:T(8,128)(2,1)S(1)}, u32[]{:S(2)}, u32[]{:S(2)}) collective-permute-start(bf16[128,128]{1,0:T(8,128)(2,1)S(1)} %get-tuple-element.251), channel_id=1, source_target_pairs={{0,24},{4,28},{1,25},{5,29},{2,26},{6,30},{3,27},{7,31}} | collective-permute-start | bytes 98312 | tf_op jit(solution)/shard_map/ppermute | solution.py:26
  91.6 8.1 %collective-permute-start.6 = (bf16[128,128]{1,0:T(8,128)(2,1)S(1)}, bf16[128,128]{1,0:T(8,128)(2,1)S(1)}, u32[]{:S(2)}, u32[]{:S(2)}) collective-permute-start(bf16[128,128]{1,0:T(8,128)(2,1)S(1)} %get-tuple-element.251), channel_id=1, source_target_pairs={{0,28},{1,29},{2,30},{3,31}} | collective-permute-start | bytes 98312 | tf_op jit(solution)/shard_map/ppermute | solution.py:26
  99.8 1.0 copy-start.5
  100.7 1.8 copy-start.1
  101.0 1.6 copy-start
  102.7 1.0 copy-start.2
  105.5 1.1 copy-start.4
  105.5 1.1 collective-permute-start.14
  106.6 8.9 %collective-permute-start.21 = (f32[128,128]{0,1:T(8,128)S(1)}, f32[128,128]{0,1:T(8,128)S(1)}, u32[]{:S(2)}, u32[]{:S(2)}) collective-permute-start(f32[128,128]{0,1:T(8,128)S(1)} %get-tuple-element.255), channel_id=1, source_target_pairs={{28,0},{29,1},{30,2},{31,3}} | collective-permute-start | bytes 196616 | tf_op jit(solution)/shard_map/ppermute | solution.py:26
  107.9 8.8 %collective-permute-start.20 = (f32[128,128]{0,1:T(8,128)S(1)}, f32[128,128]{0,1:T(8,128)S(1)}, u32[]{:S(2)}, u32[]{:S(2)}) collective-permute-start(f32[128,128]{0,1:T(8,128)S(1)} %get-tuple-element.256), channel_id=1, source_target_pairs={{24,0},{28,4},{25,1},{29,5},{26,2},{30,6},{27,3},{31,7}} | collective-permute-start | bytes 196616 | tf_op jit(solution)/shard_map/ppermute | solution.py:26
  109.2 14.3 %collective-permute-start.19 = (f32[128,128]{0,1:T(8,128)S(1)}, f32[128,128]{0,1:T(8,128)S(1)}, u32[]{:S(2)}, u32[]{:S(2)}) collective-permute-start(f32[128,128]{0,1:T(8,128)S(1)} %get-tuple-element.257), channel_id=1, source_target_pairs={{20,0},{24,4},{28,8},{21,1},{25,5},{29,9},{22,2},{26,6},{30,10},{2... | collective-permute-start | bytes 196616 | tf_op jit(solution)/shard_map/ppermute | solution.py:26
  110.5 13.0 %collective-permute-start.18 = (f32[128,128]{0,1:T(8,128)S(1)}, f32[128,128]{0,1:T(8,128)S(1)}, u32[]{:S(2)}, u32[]{:S(2)}) collective-permute-start(f32[128,128]{0,1:T(8,128)S(1)} %get-tuple-element.258), channel_id=1, source_target_pairs={{16,0},{20,4},{24,8},{28,12},{17,1},{21,5},{25,9},{29,13},{18,2},{... | collective-permute-start | bytes 196616 | tf_op jit(solution)/shard_map/ppermute | solution.py:26
  111.8 11.7 %collective-permute-start.17 = (f32[128,128]{0,1:T(8,128)S(1)}, f32[128,128]{0,1:T(8,128)S(1)}, u32[]{:S(2)}, u32[]{:S(2)}) collective-permute-start(f32[128,128]{0,1:T(8,128)S(1)} %get-tuple-element.259), channel_id=1, source_target_pairs={{12,0},{16,4},{20,8},{24,12},{28,16},{13,1},{17,5},{21,9},{25,13},... | collective-permute-start | bytes 196616 | tf_op jit(solution)/shard_map/ppermute | solution.py:26
  115.5 8.1 %collective-permute-start.16 = (f32[128,128]{0,1:T(8,128)S(1)}, f32[128,128]{0,1:T(8,128)S(1)}, u32[]{:S(2)}, u32[]{:S(2)}) collective-permute-start(f32[128,128]{0,1:T(8,128)S(1)} %get-tuple-element.260), channel_id=1, source_target_pairs={{8,0},{12,4},{16,8},{20,12},{24,16},{28,20},{9,1},{13,5},{17,9},{2... | collective-permute-start | bytes 196616 | tf_op jit(solution)/shard_map/ppermute | solution.py:26
  116.8 6.8 %collective-permute-start.15 = (f32[128,128]{0,1:T(8,128)S(1)}, f32[128,128]{0,1:T(8,128)S(1)}, u32[]{:S(2)}, u32[]{:S(2)}) collective-permute-start(f32[128,128]{0,1:T(8,128)S(1)} %get-tuple-element.254), channel_id=1, source_target_pairs={{4,0},{8,4},{12,8},{16,12},{20,16},{24,20},{28,24},{5,1},{9,5},{13... | collective-permute-start | bytes 196616 | tf_op jit(solution)/shard_map/ppermute | solution.py:26
  120.0 12.3 %all-to-all-start = ((bf16[4,128,512]{1,2,0:T(8,128)(2,1)}), bf16[4,128,512]{1,2,0:T(8,128)(2,1)S(1)}, u32[]{:S(2)}, u32[]{:S(2)}) async-start(bf16[4,128,512]{1,2,0:T(8,128)(2,1)} %stack.76), calls=%async_computation | async-start | bytes 1048576 | tf_op jit(solution)/shard_map/all_to_all | solution.py:156
  123.5 74.9 %reduce-scatter.2.cloned.1.call-start = ((), (), s32[]{:S(2)}) async-start(), calls=%async_computation.2 | async-start | bytes 589824 | tf_op jit(solution)/shard_map/reduce_scatter | solution.py:158
  124.2 74.2 %copy-start.3 = (bf16[128,64]{0,1:T(8,128)(2,1)}, bf16[128,64]{0,1:T(8,128)(2,1)S(1)}, u32[]{:S(2)}) copy-start(bf16[128,64]{0,1:T(8,128)(2,1)S(1)} %get-tuple-element.262) | copy-start | bytes 49156
Sparse Core Ops, SparseCore 0:
  133.5 64.8 reduce-scatter.1
